TPU v7x, 32 devices: a whole 2x2x4 slice. The times are simulated.
32 devices in a mesh: grp: 2 (over y), sp: 4 (over z), tp: 4 (over x, core).
Axes of the slice: x: 2, y: 2, z: 4, core: 2. Of those that a mesh axis runs over, the one named last changes fastest.
Arguments:
- tokens: bfloat16 [8192, 2048], P(('grp', 'sp', 'tp')), parts along dimension 0, may hold values from -6 to 6
- step: float32 [8192], P(('grp', 'sp')), parts along dimension 0, may hold values from 0.2 to 3.75
- in_gain: float32 [2048], replicated, may hold values from 0.1 to 1.9
- in_proj: bfloat16 [2048, 512], P(None, 'tp'), may hold values from -0.125 to 0.125
- decay_rate: float32 [32, 64], P('tp'), may hold values from 2.4414063e-05 to 0.04
- frequency: float32 [32, 64], P('tp'), may hold values from 0.2 to 3
- input_map: float32 [2, 32, 64, 16], P(None, 'tp'), may hold values from -1 to 1
- readout: float32 [2, 32, 16, 64], P(None, 'tp'), may hold values from -0.75 to 0.75
- out_gain: float32 [512], replicated, may hold values from 0.1 to 1.9
- out_proj: bfloat16 [512, 2048], replicated, may hold values from -0.25 to 0.25
Outputs:
- mixed: bfloat16 [8192, 2048], P(('grp', 'sp', 'tp')), parts along dimension 0
There are 2 independent parts, one for each index of `grp`. A program takes and returns all parts, laid end to end along the dimension named above; an argument that names none is the same for every part. Nothing has to cross between parts.
All inputs are finite; a program needn't handle non-finite values.
Results may differ from a plain program's by a relative error of at most 0.01.
Values may be sent and summed in bfloat16 or wider, within the bound.
A program may use at most 64 MiB of HBM per device.

v0:
```python
from functools import partial

import jax
import jax.numpy as jnp
from jax import lax
from jax.sharding import PartitionSpec as P

SPAN = 64


HIGHEST = lax.Precision.HIGHEST


def prefix(value, axis, join, neutral):
    count, mine = (lax.axis_size(axis), lax.axis_index(axis))
    pieces = jax.tree.map(lambda part: lax.all_gather(part, axis), value)
    so_far = jax.tree.map(
        lambda part, zero: jnp.full_like(part, 0) + jnp.asarray(zero, part.dtype), value, neutral
    )

    def lap(position, so_far):
        longer = join(so_far, jax.tree.map(lambda part: part[position], pieces))
        return jax.tree.map(lambda new, old: jnp.where(position < mine, new, old), longer, so_far)

    return lax.fori_loop(0, count - 1, lap, so_far)


def compose(earlier, later):
    a_re, a_im, b_re, b_im = earlier
    c_re, c_im, d_re, d_im = later
    return (
        c_re * a_re - c_im * a_im,
        c_re * a_im + c_im * a_re,
        c_re * b_re - c_im * b_im + d_re,
        c_re * b_im + c_im * b_re + d_im,
    )


def rms_rows(values, gain):
    values = values.astype(jnp.float32)
    scaled = values * lax.rsqrt(jnp.mean(values * values, axis=-1, keepdims=True) + 1e-06)
    return (scaled * gain).astype(jnp.bfloat16)


def block_tables(input_map, readout):
    groups = input_map.shape[1]
    unit = jnp.eye(groups, dtype=jnp.float32)
    push_re = jnp.einsum("gph,gk->ghkp", input_map[0], unit, precision=HIGHEST)
    push_im = jnp.einsum("gph,gk->ghkp", input_map[1], unit, precision=HIGHEST)
    read_re = jnp.einsum("ghp,gk->gpkh", readout[0], unit, precision=HIGHEST)
    read_im = jnp.einsum("ghp,gk->gpkh", readout[1], unit, precision=HIGHEST)
    inner = push_re.shape[0] * push_re.shape[1]
    flat = push_re.shape[2] * push_re.shape[3]
    return (
        push_re.reshape(inner, flat),
        push_im.reshape(inner, flat),
        read_re.reshape(flat, inner),
        read_im.reshape(flat, inner),
    )


def response(s_re, s_im, read_re, read_im):
    value = jnp.dot(s_re, read_re, precision=HIGHEST) - jnp.dot(s_im, read_im, precision=HIGHEST)
    return jax.nn.gelu(value, approximate=True).astype(jnp.bfloat16)


def advance(carry, piece, rates, freqs, tables, lower, keep):
    drive_part, time_part = piece
    push_re, push_im, read_re, read_im = tables
    own = time_part[:, None]
    magnitude = jnp.exp(-rates[None] * own)
    a_re = magnitude * jnp.cos(freqs[None] * own)
    a_im = magnitude * jnp.sin(freqs[None] * own)
    lam_re = -rates
    denom = lam_re * lam_re + freqs * freqs
    n_re = a_re - 1.0
    z_re = (n_re * lam_re + a_im * freqs) / denom
    z_im = (a_im * lam_re - n_re * freqs) / denom
    grouped = drive_part.astype(jnp.float32)
    in_re = jnp.dot(grouped, push_re, precision=HIGHEST)
    in_im = jnp.dot(grouped, push_im, precision=HIGHEST)
    i_re = z_re * in_re - z_im * in_im
    i_im = z_re * in_im + z_im * in_re
    elapsed = jnp.dot(lower, time_part, precision=HIGHEST)[:, None]
    grow = jnp.exp(rates[None] * elapsed)
    angle = freqs[None] * elapsed
    cosine = jnp.cos(angle)
    sine = jnp.sin(angle)
    w_re = grow * (cosine * i_re + sine * i_im)
    w_im = grow * (cosine * i_im - sine * i_re)
    acc_re = jnp.dot(lower, w_re, precision=HIGHEST)
    acc_im = jnp.dot(lower, w_im, precision=HIGHEST)
    shrink = jnp.exp(-rates[None] * elapsed)
    c_re = shrink * cosine
    c_im = shrink * sine
    s_re = c_re * acc_re - c_im * acc_im
    s_im = c_re * acc_im + c_im * acc_re
    d_re, d_im, e_re, e_im = carry
    full_re = s_re + c_re * e_re - c_im * e_im
    full_im = s_im + c_re * e_im + c_im * e_re
    cum_re = c_re * d_re - c_im * d_im
    cum_im = c_re * d_im + c_im * d_re
    ends = (cum_re[-1], cum_im[-1], full_re[-1], full_im[-1])
    return (ends, (cum_re, cum_im, full_re, full_im))


def on_device(
    tokens, step, in_gain, in_proj, decay_rate, frequency, input_map, readout, out_gain, out_proj
):
    normed = rms_rows(tokens, in_gain)
    rates, freqs, maps, reads = (decay_rate, frequency, input_map, readout)
    drive = jnp.dot(
        lax.all_gather(normed, "tp", axis=0, tiled=True),
        in_proj,
        preferred_element_type=jnp.float32,
    ).astype(jnp.bfloat16)
    tables = block_tables(maps, reads)
    flat_rates = rates.reshape(-1)
    flat_freqs = freqs.reshape(-1)
    seq_rows = drive.shape[0]
    block_count = seq_rows // SPAN
    drive_blocks = drive.reshape(block_count, SPAN, -1)
    time_blocks = step.reshape(block_count, SPAN)
    rows_index = lax.broadcasted_iota(jnp.int32, (SPAN, SPAN), 0)
    cols_index = lax.broadcasted_iota(jnp.int32, (SPAN, SPAN), 1)
    lower = (cols_index <= rows_index).astype(jnp.float32)
    zeros = jnp.zeros(flat_rates.shape, jnp.float32)
    ones = jnp.ones(flat_rates.shape, jnp.float32)
    start_carry = (ones, zeros, zeros, zeros)
    keep_first = "states"
    ends, stored = lax.scan(
        partial(
            advance, rates=flat_rates, freqs=flat_freqs, tables=tables, lower=lower, keep=keep_first
        ),
        start_carry,
        (drive_blocks, time_blocks),
    )
    incoming = prefix(ends, "sp", compose, start_carry)
    cum_re, cum_im, full_re, full_im = stored
    width = flat_rates.shape[0]
    cum_re = cum_re.reshape(seq_rows, width)
    cum_im = cum_im.reshape(seq_rows, width)
    state_re = full_re.reshape(seq_rows, width) + cum_re * incoming[2] - cum_im * incoming[3]
    state_im = full_im.reshape(seq_rows, width) + cum_re * incoming[3] + cum_im * incoming[2]
    answer = response(state_re, state_im, tables[2], tables[3])
    gathered = lax.all_to_all(answer, "tp", split_axis=0, concat_axis=1, tiled=True)
    shaped = rms_rows(gathered, out_gain)
    return jnp.dot(shaped, out_proj, preferred_element_type=jnp.float32).astype(jnp.bfloat16)


def solution(mesh):
    placed = (
        P(("grp", "sp", "tp"), None),
        P(("grp", "sp")),
        P(),
        P(None, "tp"),
        P("tp", None),
        P("tp", None),
        P(None, "tp", None, None),
        P(None, "tp", None, None),
        P(),
        P(),
    )
    return jax.shard_map(
        on_device,
        mesh=mesh,
        in_specs=placed,
        out_specs=P(("grp", "sp", "tp"), None),
        check_vma=False,
    )
```

profile of v0, /device:TPU:0, one launch (start us, length us, event | category | flops | bytes accessed | tf_op | source)
XLA Modules:
  0.0 303.8 jit_solution(8982933017451416481)
XLA Ops:
  15.6 32.5 %all-gather.10.cloned.1.call-done = bf16[1024,2048]{1,0:T(8,128)(2,1)} async-done(((bf16[256,2048]{1,0:T(8,128)(2,1)}), bf16[1024,2048]{1,0:T(8,128)(2,1)}) %all-gather.10.cloned.1.call-update) | async-done | bytes 4194320 | tf_op jit(solution)/shard_map/all_gather | solution.py:113
  48.1 4.3 %convolution_convert_fusion.1 = bf16[1024,128]{1,0:T(8,128)(2,1)} fusion(bf16[1024,2048]{1,0:T(8,128)(2,1)} %all-gather.10.cloned.1.call-done, bf16[2048,128]{1,0:T(8,128)(2,1)} %param.17), kind=kOutput, calls=%fused_computation.81 | convolution fusion | flops 537001984 | bytes 4980736 | tf_op jit(solution)/shard_map/dot_general | solution.py:112
  53.6 173.3 %while.48 = (s32[]{:T(128)}, f32[512]{0:T(512)S(1)}, f32[512]{0:T(512)S(1)}, f32[512]{0:T(512)}, f32[512]{0:T(512)}, /*index=5*/f32[16,64,512]{2,1,0:T(8,128)}, ...) while((s32[]{:T(128)}, f32[512]{0:T(512)S(1)}, ...), condition=%wide.wide.region_2.3_spmd.clone.clone.clone, body=%wide.wide.region_1.2_spmd.clone.clone.clone.sunk | while | flops 153889792 | bytes 4405837 | solution.py:131
  59.6 3.0 add_dynamic-update-slice_fusion.3
  70.4 3.0 add_dynamic-update-slice_fusion.3
  81.3 3.0 add_dynamic-update-slice_fusion.3
  92.1 3.0 add_dynamic-update-slice_fusion.3
  102.9 3.0 add_dynamic-update-slice_fusion.3
  113.7 3.0 add_dynamic-update-slice_fusion.3
  124.6 3.0 add_dynamic-update-slice_fusion.3
  135.4 3.0 add_dynamic-update-slice_fusion.3
  146.2 3.0 add_dynamic-update-slice_fusion.3
  157.1 3.0 add_dynamic-update-slice_fusion.3
  189.6 3.0 add_dynamic-update-slice_fusion.3
  200.4 3.0 add_dynamic-update-slice_fusion.3
  211.3 3.0 add_dynamic-update-slice_fusion.3
  222.1 3.0 add_dynamic-update-slice_fusion.3
  226.9 12.2 %all-gather.7 = f32[4,1,512]{2,1,0:T(1,128)S(1)} all-gather(f32[1,1,512]{2,1,0:T(1,128)} %bitcast.171), channel_id=5, replica_groups=mesh['grp'=2,'sp'=4,'tp'=4] {'sp'}, dimensions={0}, use_global_device_ids=true | all-gather | bytes 10240 | tf_op jit(solution)/shard_map/all_gather | solution.py:16
  239.1 12.1 %all-gather.6 = f32[4,1,512]{2,1,0:T(1,128)S(1)} all-gather(f32[1,1,512]{2,1,0:T(1,128)} %bitcast.169), channel_id=4, replica_groups=mesh['grp'=2,'sp'=4,'tp'=4] {'sp'}, dimensions={0}, use_global_device_ids=true | all-gather | bytes 10240 | tf_op jit(solution)/shard_map/all_gather | solution.py:16
  251.2 11.9 %all-gather.5 = f32[4,1,512]{2,1,0:T(1,128)S(1)} all-gather(f32[1,1,512]{2,1,0:T(1,128)S(1)} %bitcast.160), channel_id=3, replica_groups=mesh['grp'=2,'sp'=4,'tp'=4] {'sp'}, dimensions={0}, use_global_device_ids=true | all-gather | bytes 10240 | tf_op jit(solution)/shard_map/all_gather | solution.py:16
  263.2 12.1 %all-gather.4 = f32[4,1,512]{2,1,0:T(1,128)S(1)} all-gather(f32[1,1,512]{2,1,0:T(1,128)S(1)} %bitcast.158), channel_id=2, replica_groups=mesh['grp'=2,'sp'=4,'tp'=4] {'sp'}, dimensions={0}, use_global_device_ids=true | all-gather | bytes 10240 | tf_op jit(solution)/shard_map/all_gather | solution.py:16
  275.3 3.2 %while.47 = (s32[]{:T(128)}, f32[512]{0:T(512)}, f32[512]{0:T(512)}, s32[]{:T(128)}, f32[4,512]{1,0:T(4,128)S(1)}, /*index=5*/f32[4,512]{1,0:T(4,128)S(1)}, f32[...) while((s32[]{:T(128)}, f32[512]{0:T(512)}, f32[512]{0:T(512)}, s32[]{:T(128)}, ...), condition=%wide.region_4.5_spmd.clone, body=%wide.region_3.4_spmd.clone.sunk | while | flops 6148 | bytes 32897 | solution.py:25
  278.5 4.3 %multiply_add_fusion.5 = (f32[16,64,512]{2,1,0:T(8,128)S(1)}, f32[16,64,512]{2,1,0:T(8,128)S(1)}) fusion(f32[16,64,512]{2,1,0:T(8,128)} %get-tuple-element.435, f32[16,64,512]{2,1,0:T(8,128)} %get-tuple-element.437, f32[16,64,512]{2,1,0:T(8,128)} %get-tuple-element.429, f32[512]{0:T(512)} %get-tuple-element.436, f32[512]{0:T(512)} %get-tuple-element.434, ...), kind=kLoop, calls=%fused_computation.78 | loop fusion | flops 4194304 | bytes 12587008 | tf_op jit(solution)/shard_map/add | solution.py:144
  286.6 8.4 %all_to_all.13 = bf16[4,256,128]{1,2,0:T(8,128)(2,1)S(1)} all-to-all(bf16[4,256,128]{1,2,0:T(8,128)(2,1)S(1)} %copy.20), channel_id=1, replica_groups=mesh['grp'=2,'sp'=4,'tp'=4] {'tp'}, dimensions={0} | all-to-all | bytes 524288 | tf_op jit(solution)/shard_map/all_to_all | solution.py:146
  (454 shorter events, 147.7 us)
Async XLA Ops:
  6.5 288.7 %copy-start = (bf16[512,2048]{1,0:T(8,128)(2,1)S(1)}, bf16[512,2048]{1,0:T(8,128)(2,1)}, u32[]{:S(2)}) copy-start(bf16[512,2048]{1,0:T(8,128)(2,1)} %param.23) | copy-start | bytes 6291460
  6.5 6.3 %copy-start.10 = (f32[1024]{0:T(1024)S(1)}, f32[1024]{0:T(1024)}, u32[]{:S(2)}) copy-start(f32[1024]{0:T(1024)} %param.15) | copy-start | bytes 12292
  6.5 6.9 %copy-start.3 = (f32[2,8,16,64]{3,2,1,0:T(8,128)S(1)}, f32[2,8,16,64]{3,2,1,0:T(8,128)}, u32[]{:S(2)}) copy-start(f32[2,8,16,64]{3,2,1,0:T(8,128)} %param.21) | copy-start | bytes 196612
  6.5 41.6 %all-gather.10.cloned.1.call-start = ((), (), s32[]{:S(2)}) async-start(), calls=%async_computation.1 | async-start | bytes 5242880 | tf_op jit(solution)/shard_map/all_gather | solution.py:113
  140.5 5.7 %copy-start.5 = (f32[1,512]{1,0:T(1,128)S(1)}, f32[1,512]{1,0:T(1,128)}, u32[]{:S(2)}) copy-start(f32[1,512]{1,0:T(1,128)} %get-tuple-element.1020) | copy-start | bytes 6148 | tf_op jit(solution)/shard_map/while
  140.5 5.7 %copy-start.8 = (f32[512]{0:T(512)S(1)}, f32[512]{0:T(512)}, u32[]{:S(2)}) copy-start(f32[512]{0:T(512)} %get-tuple-element.993) | copy-start | bytes 6148 | tf_op jit(solution)/shard_map/while
  140.5 5.7 %copy-start.9 = (f32[512]{0:T(512)S(1)}, f32[512]{0:T(512)}, u32[]{:S(2)}) copy-start(f32[512]{0:T(512)} %get-tuple-element.994) | copy-start | bytes 6148 | tf_op jit(solution)/shard_map/while
  140.5 5.7 %copy-start.12 = (f32[512]{0:T(512)S(1)}, f32[512]{0:T(512)}, u32[]{:S(2)}) copy-start(f32[512]{0:T(512)} %get-tuple-element.1030) | copy-start | bytes 6148 | tf_op jit(solution)/shard_map/while
  140.5 5.7 %copy-start.13 = (f32[1,512]{1,0:T(1,128)S(1)}, f32[1,512]{1,0:T(1,128)}, u32[]{:S(2)}) copy-start(f32[1,512]{1,0:T(1,128)} %get-tuple-element.1024) | copy-start | bytes 6148 | tf_op jit(solution)/shard_map/while
  151.3 5.7 %copy-start.5 = (f32[1,512]{1,0:T(1,128)S(1)}, f32[1,512]{1,0:T(1,128)}, u32[]{:S(2)}) copy-start(f32[1,512]{1,0:T(1,128)} %get-tuple-element.1020) | copy-start | bytes 6148 | tf_op jit(solution)/shard_map/while
  151.3 5.7 %copy-start.8 = (f32[512]{0:T(512)S(1)}, f32[512]{0:T(512)}, u32[]{:S(2)}) copy-start(f32[512]{0:T(512)} %get-tuple-element.993) | copy-start | bytes 6148 | tf_op jit(solution)/shard_map/while
  151.3 5.7 %copy-start.9 = (f32[512]{0:T(512)S(1)}, f32[512]{0:T(512)}, u32[]{:S(2)}) copy-start(f32[512]{0:T(512)} %get-tuple-element.994) | copy-start | bytes 6148 | tf_op jit(solution)/shard_map/while
  151.4 5.7 %copy-start.12 = (f32[512]{0:T(512)S(1)}, f32[512]{0:T(512)}, u32[]{:S(2)}) copy-start(f32[512]{0:T(512)} %get-tuple-element.1030) | copy-start | bytes 6148 | tf_op jit(solution)/shard_map/while
  183.8 5.7 %copy-start.5 = (f32[1,512]{1,0:T(1,128)S(1)}, f32[1,512]{1,0:T(1,128)}, u32[]{:S(2)}) copy-start(f32[1,512]{1,0:T(1,128)} %get-tuple-element.1020) | copy-start | bytes 6148 | tf_op jit(solution)/shard_map/while
  183.8 5.7 %copy-start.8 = (f32[512]{0:T(512)S(1)}, f32[512]{0:T(512)}, u32[]{:S(2)}) copy-start(f32[512]{0:T(512)} %get-tuple-element.993) | copy-start | bytes 6148 | tf_op jit(solution)/shard_map/while
  183.9 5.7 %copy-start.9 = (f32[512]{0:T(512)S(1)}, f32[512]{0:T(512)}, u32[]{:S(2)}) copy-start(f32[512]{0:T(512)} %get-tuple-element.994) | copy-start | bytes 6148 | tf_op jit(solution)/shard_map/while
  183.9 5.7 %copy-start.12 = (f32[512]{0:T(512)S(1)}, f32[512]{0:T(512)}, u32[]{:S(2)}) copy-start(f32[512]{0:T(512)} %get-tuple-element.1030) | copy-start | bytes 6148 | tf_op jit(solution)/shard_map/while
  183.9 5.7 %copy-start.13 = (f32[1,512]{1,0:T(1,128)S(1)}, f32[1,512]{1,0:T(1,128)}, u32[]{:S(2)}) copy-start(f32[1,512]{1,0:T(1,128)} %get-tuple-element.1024) | copy-start | bytes 6148 | tf_op jit(solution)/shard_map/while
  205.5 5.7 %copy-start.5 = (f32[1,512]{1,0:T(1,128)S(1)}, f32[1,512]{1,0:T(1,128)}, u32[]{:S(2)}) copy-start(f32[1,512]{1,0:T(1,128)} %get-tuple-element.1020) | copy-start | bytes 6148 | tf_op jit(solution)/shard_map/while
  205.5 5.7 %copy-start.8 = (f32[512]{0:T(512)S(1)}, f32[512]{0:T(512)}, u32[]{:S(2)}) copy-start(f32[512]{0:T(512)} %get-tuple-element.993) | copy-start | bytes 6148 | tf_op jit(solution)/shard_map/while
  205.5 5.7 %copy-start.9 = (f32[512]{0:T(512)S(1)}, f32[512]{0:T(512)}, u32[]{:S(2)}) copy-start(f32[512]{0:T(512)} %get-tuple-element.994) | copy-start | bytes 6148 | tf_op jit(solution)/shard_map/while
  205.5 5.7 %copy-start.12 = (f32[512]{0:T(512)S(1)}, f32[512]{0:T(512)}, u32[]{:S(2)}) copy-start(f32[512]{0:T(512)} %get-tuple-element.1030) | copy-start | bytes 6148 | tf_op jit(solution)/shard_map/while
  205.6 5.7 %copy-start.13 = (f32[1,512]{1,0:T(1,128)S(1)}, f32[1,512]{1,0:T(1,128)}, u32[]{:S(2)}) copy-start(f32[1,512]{1,0:T(1,128)} %get-tuple-element.1024) | copy-start | bytes 6148 | tf_op jit(solution)/shard_map/while
  284.6 10.5 %copy-start.11 = (f32[512]{0:T(512)S(1)}, f32[512]{0:T(512)}, u32[]{:S(2)}) copy-start(f32[512]{0:T(512)} %param.22) | copy-start | bytes 6148
  (66 other events, 367.4 us)
Sparse Core Ops, SparseCore 0:
  10.9 37.1 all-gather.9
where the time goes:
time: 309 us; the launch traced here: 304 us
  matrix products  134 us (43%)
  blocking collectives  56.8 us (18%)
  local copies, waits for them, and re-layouts  40.9 us (13%)
  waiting for transfers between devices  32.6 us (11%)
  other arithmetic  23.6 us (8%)
  between operations  13.6 us (4%)
    all_gather x4, blocking collectives, prefix(): pieces = jax.tree.map(lambda part: lax.all_gather(part, axis), value)  48.4 us
    dot_general x16, matrix products, advance(): acc_im = jnp.dot(lower, w_im, precision=HIGHEST)  47.9 us
    all_gather x1, waiting for transfers between devices, on_device(): lax.all_gather(normed, 'tp', axis=0, tiled=True)  32.5 us
    dot_general x16, matrix products, advance(): acc_re = jnp.dot(lower, w_re, precision=HIGHEST)  32.3 us
    slice x32, local copies, waits for them, and re-layouts, advance(): ends = (cum_re[-1], cum_im[-1], full_re[-1], full_im[-1])  18.8 us
    dot_general x16, matrix products, advance(): in_im = jnp.dot(grouped, push_im, precision=HIGHEST)  15.3 us
    dot_general x16, matrix products, advance(): in_re = jnp.dot(grouped, push_re, precision=HIGHEST)  15.3 us
    dot_general x16, matrix products, advance(): elapsed = jnp.dot(lower, time_part, precision=HIGHEST)[:, None]  13.1 us
  transfers between devices with their start and end apart: 1, of which 1 were waited for; matrix products, arithmetic and copies ran while one was open for 2% of the time, Pallas kernels for 0%

commit v1 on v0

v1 whole, which is shorter than its diff:
```python
import functools
import math

import jax
import jax.numpy as jnp
from jax import lax
from jax.experimental import pallas as pl
from jax.experimental.pallas import tpu as pltpu
from jax.sharding import PartitionSpec as P

F32 = jnp.float32
BF16 = jnp.bfloat16
MESH = pl.DeviceIdType.MESH
CHUNKS = 4
STRIP = 16
COLS = 512
COS = (0.9999992107823232, -19.738980355764078, 64.9286574210355, -85.2716215343227, 58.79049212023138, -21.071105627794083)
SIN = (6.28318491649543, -41.34158923268886, 81.59994332979169, -76.61447253134615, 41.34288235500672, -12.471243535733244)
FORM = dict(preferred_element_type=F32)


def poly(coefs, z):
    total = coefs[-1] * z + coefs[-2]
    for value in coefs[-3::-1]:
        total = total * z + value
    return total


def turn(phase):
    r = phase - jnp.round(phase)
    z = r * r
    return poly(COS, z), poly(SIN, z) * r


def kernel(
    n, n_tp, tok_hbm, step_ref, gain_ref, proj_hbm, rf_ref, bc_ref, ogain_ref, oproj_hbm, out_ref,
    tok, normed, w_in, oproj, p_re, p_im, d_re, d_im, p_cat, y_loc,
    wide, acc, state, times, rf_all, bc_all, rf8, e_send, e_recv, dt_send, dt_recv,
    c_w, s_w, x_ref, tab, shaped,
    load_sem, small_sem, small_send, w_recv, w_send, bc_recv, bc_send,
    e_rsem, e_ssem, dt_rsem, dt_ssem,
):
    grp, sp, tp = lax.axis_index("grp"), lax.axis_index("sp"), lax.axis_index("tp")
    rank = sp * n_tp + tp
    rows = tok.shape[0]
    depth = w_in.shape[1]
    half = depth // 2
    piece = half // CHUNKS
    lanes = rf_all.shape[-1]
    blocks = lanes // 128

    def place(r):
        return {"sp": r // n_tp, "tp": lax.rem(r, n_tp)}

    peer = [None] + [{"tp": tp ^ m} for m in range(1, n_tp)]
    across = {"grp": 1 - grp}

    loads = [
        pltpu.make_async_copy(proj_hbm, w_in.at[0], load_sem.at[0]),
        pltpu.make_async_copy(tok_hbm, tok, load_sem.at[1]),
        pltpu.make_async_copy(oproj_hbm, oproj, load_sem.at[2]),
    ]
    for copy in loads:
        copy.start()

    barrier = pltpu.get_barrier_semaphore()

    def greet(k, _):
        pl.semaphore_signal(barrier, inc=1, device_id=place(lax.rem(rank + k, n)), device_id_type=MESH)
        return 0

    lax.fori_loop(1, n, greet, 0)
    pl.semaphore_signal(barrier, inc=1, device_id=across, device_id_type=MESH)

    step_row = step_ref[...]
    row_id = lax.broadcasted_iota(jnp.int32, (rows, rows), 0)
    col_id = lax.broadcasted_iota(jnp.int32, (rows, rows), 1)
    causal = col_id <= row_id
    elapsed = jnp.sum(jnp.where(causal, jnp.broadcast_to(step_row, (rows, rows)), 0.0), axis=1, keepdims=True)
    times[...] = jnp.broadcast_to(elapsed, (rows, 128))
    dt_send[...] = jnp.broadcast_to(jnp.sum(step_row, axis=1, keepdims=True), (1, 128))
    lower = causal.astype(F32).astype(BF16)

    loads[0].wait()
    pl.semaphore_wait(barrier, n)

    started = []

    def send(src, dst, ssem, rsem, where):
        copy = pltpu.make_async_remote_copy(
            src_ref=src, dst_ref=dst, send_sem=ssem, recv_sem=rsem, device_id=where, device_id_type=MESH
        )
        copy.start()
        started.append(copy)
        return copy

    def arrived(dst, rsem):
        pltpu.make_async_copy(dst, dst, rsem).wait()

    for m in range(1, n_tp):
        send(rf_ref, rf_all.at[m], small_send.at[m], small_sem.at[m], peer[m])
    own_half = grp * half
    other_half = (1 - grp) * half
    for c in range(CHUNKS):
        part = pl.ds(pl.multiple_of(own_half + c * piece, 128), piece)
        send(w_in.at[0, part], w_in.at[2, part], w_send.at[0, c], w_recv.at[0, c], peer[2])
    send(w_in.at[0], w_in.at[1], w_send.at[1, 0], w_recv.at[1, 0], peer[1])
    send(bc_ref.at[grp], bc_all.at[2, grp], bc_send.at[0], bc_recv.at[0], peer[2])
    send(bc_ref, bc_all.at[1], bc_send.at[1], bc_recv.at[1], peer[1])

    def send_times(r, _):
        copy = pltpu.make_async_remote_copy(
            src_ref=dt_send, dst_ref=dt_recv.at[rank], send_sem=dt_ssem.at[r], recv_sem=dt_rsem.at[rank],
            device_id=place(r), device_id_type=MESH,
        )
        copy.start()
        return 0

    lax.fori_loop(rank + 1, n, send_times, 0)

    rf_all[0] = rf_ref[...]
    bc_all[0] = bc_ref[...]

    loads[1].wait()
    gain = gain_ref[...]

    def norm_strip(i, _):
        at = pl.ds(pl.multiple_of(i * STRIP, STRIP), STRIP)
        value = tok[at, :].astype(F32)
        scale = lax.rsqrt(jnp.mean(value * value, axis=1, keepdims=True) + 1e-6)
        normed[at, :] = (value * scale * gain).astype(BF16)
        return 0

    lax.fori_loop(0, rows // STRIP, norm_strip, 0)

    def forward(c, mine):
        base = own_half if mine else other_half
        part = pl.ds(pl.multiple_of(base + c * piece, 128), piece)
        way = 0 if mine else 2
        arrived(w_in.at[2, part], w_recv.at[way, c])
        if mine:
            send(w_in.at[2, part], w_in.at[2, part], w_send.at[2, c], w_recv.at[2, c], across)
        send(w_in.at[2, part], w_in.at[3, part], w_send.at[3 if mine else 4, c], w_recv.at[3 if mine else 4, c], peer[1])

    def tables(m):
        rate = rf_all[m, 0:1, :]
        freq = rf_all[m, 1:2, :]
        first = lax.broadcasted_iota(jnp.int32, (STRIP, lanes), 0) == 0

        def strip(i, before):
            br, bi = before
            at = pl.ds(pl.multiple_of(i * STRIP, STRIP), STRIP)
            t = times[at, 0:1]
            c, s = turn(t * freq)
            load = t * rate
            small = jnp.exp(-load)
            large = jnp.exp(load)
            pr, pi = small * c, small * s
            p_re[m, at, :] = pr
            p_im[m, at, :] = pi
            p_cat[m, at, 0:lanes] = pr.astype(BF16)
            p_cat[m, at, lanes:] = pi.astype(BF16)
            qr, qi = large * c, -large * s
            d_re[m, at, :] = jnp.where(first, pltpu.roll(br, 1, 0), pltpu.roll(qr, 1, 0)) - qr
            d_im[m, at, :] = jnp.where(first, pltpu.roll(bi, 1, 0), pltpu.roll(qi, 1, 0)) - qi
            return qr, qi

        lax.fori_loop(0, rows // STRIP, strip, (jnp.ones((STRIP, lanes), F32), jnp.zeros((STRIP, lanes), F32)))

    per = 16
    mask_r = lax.broadcasted_iota(jnp.int32, (128, lanes), 0) // per
    mask_c = lax.broadcasted_iota(jnp.int32, (128, lanes), 1) // (lanes // (128 // per))
    same = mask_r == mask_c

    def spread(compact):
        return jnp.where(same, jnp.concatenate([compact.astype(F32)] * (128 // per), axis=0), 0.0)

    def local(m):
        tab[:, 0:lanes] = spread(bc_all[m, 0, 0]).astype(BF16)
        tab[:, lanes:] = spread(bc_all[m, 0, 1]).astype(BF16)
        drive = jnp.dot(normed[...], w_in[m], **FORM).astype(BF16)
        acc[...] = jnp.dot(drive, tab[...], **FORM)

        def weigh(i, _):
            at = pl.ds(pl.multiple_of(i * STRIP, STRIP), STRIP)
            vr, vi = acc[at, 0:lanes], acc[at, lanes:]
            dr, di = d_re[m, at, :], d_im[m, at, :]
            wide[at, 0:lanes] = (dr * vr - di * vi).astype(BF16)
            wide[at, lanes:] = (dr * vi + di * vr).astype(BF16)
            return 0

        lax.fori_loop(0, rows // STRIP, weigh, 0)
        acc[...] = jnp.dot(lower, wide[...], **FORM)
        last = pl.ds(rows - 1, 1)
        for b in range(blocks):
            at = pl.ds(b * 128, 128)
            ar, ai = acc[last, at], acc[last, pl.ds(lanes + b * 128, 128)]
            pr, pi = p_re[m, last, at], p_im[m, last, at]
            e_send[m, pl.ds(b, 1), :] = pr * ar - pi * ai
            e_send[m, pl.ds(blocks + b, 1), :] = pr * ai + pi * ar
        owner = tp ^ m

        def send_end(r, _):
            copy = pltpu.make_async_remote_copy(
                src_ref=e_send.at[m], dst_ref=e_recv.at[rank, owner], send_sem=e_ssem.at[r, m],
                recv_sem=e_rsem.at[rank, owner], device_id=place(r), device_id_type=MESH,
            )
            copy.start()
            return 0

        lax.fori_loop(rank + 1, n, send_end, 0)

        def rotate(i, _):
            at = pl.ds(pl.multiple_of(i * STRIP, STRIP), STRIP)
            ar, ai = acc[at, 0:lanes], acc[at, lanes:]
            pr, pi = p_re[m, at, :], p_im[m, at, :]
            state[at, 0:lanes] = (pr * ar - pi * ai).astype(BF16)
            state[at, lanes:] = (pr * ai + pi * ar).astype(BF16)
            return 0

        lax.fori_loop(0, rows // STRIP, rotate, 0)
        tab[:, 0:lanes] = spread(bc_all[m, 1, 0]).astype(BF16)
        tab[:, lanes:] = (-spread(bc_all[m, 1, 1])).astype(BF16)
        y_loc[m] = lax.dot_general(state[...], tab[...], (((1,), (1,)), ((), ())), **FORM)

    tables(0)
    local(0)
    for m in range(1, n_tp):
        arrived(rf_all.at[m], small_sem.at[m])
    tables(1)
    for c in range(CHUNKS):
        forward(c, True)
    arrived(bc_all.at[2, grp], bc_recv.at[0])
    send(bc_all.at[2, grp], bc_all.at[2, grp], bc_send.at[2], bc_recv.at[2], across)
    send(bc_all.at[2, grp], bc_all.at[3, grp], bc_send.at[3], bc_recv.at[3], peer[1])
    tables(2)
    for c in range(CHUNKS):
        forward(c, False)
    arrived(bc_all.at[2, 1 - grp], bc_recv.at[2])
    send(bc_all.at[2, 1 - grp], bc_all.at[3, 1 - grp], bc_send.at[4], bc_recv.at[4], peer[1])
    arrived(w_in.at[1], w_recv.at[1, 0])
    arrived(bc_all.at[1], bc_recv.at[1])
    local(1)
    tables(3)
    local(2)
    sign = jnp.where(lax.broadcasted_iota(jnp.int32, (2 * blocks, 128), 0) < blocks, -1.0, 1.0)
    for m in range(n_tp):
        for b in range(blocks):
            at = pl.ds(b * 128, 128)
            for kind in range(2):
                value = rf_all[m, kind:kind + 1, at]
                rf8[m, kind, pl.ds(b, 1), :] = value
                rf8[m, kind, pl.ds(blocks + b, 1), :] = value

    def weight(k, since):
        j = rank - 1 - k
        arrived(dt_recv.at[j], dt_rsem.at[j])
        for m in range(n_tp):
            c, s = turn(since * rf8[m, 1])
            shrink = jnp.exp(-since * rf8[m, 0])
            c_w[j, m] = shrink * c
            s_w[j, m] = shrink * s * sign
        return since + dt_recv[j]

    lax.fori_loop(0, rank, weight, jnp.zeros((1, 128), F32))

    for c in range(CHUNKS):
        arrived(w_in.at[3, pl.ds(pl.multiple_of(own_half + c * piece, 128), piece)], w_recv.at[3, c])
        arrived(w_in.at[3, pl.ds(pl.multiple_of(other_half + c * piece, 128), piece)], w_recv.at[4, c])
    arrived(bc_all.at[3, grp], bc_recv.at[3])
    arrived(bc_all.at[3, 1 - grp], bc_recv.at[4])
    local(3)

    total = jnp.zeros((rows, 1), F32)
    for m in range(n_tp):
        owner = tp ^ m

        def take(j, x):
            arrived(e_recv.at[j, owner], e_rsem.at[j, owner])
            value = e_recv[j, owner]
            return x + c_w[j, m] * value + s_w[j, m] * pltpu.roll(value, blocks, 0)

        x_ref[...] = lax.fori_loop(0, rank, take, jnp.zeros((2 * blocks, 128), F32))
        cr = spread(bc_all[m, 1, 0])
        ci = spread(bc_all[m, 1, 1])
        for b in range(blocks):
            at = slice(b * 128, (b + 1) * 128)
            xr, xi = x_ref[pl.ds(b, 1), :], x_ref[pl.ds(blocks + b, 1), :]
            tab[:, b * 128:(b + 1) * 128] = (cr[:, at] * xr - ci[:, at] * xi).astype(BF16)
            tab[:, lanes + b * 128:lanes + (b + 1) * 128] = (-(cr[:, at] * xi + ci[:, at] * xr)).astype(BF16)
        v = y_loc[m] + lax.dot_general(p_cat[m], tab[...], (((1,), (1,)), ((), ())), **FORM)
        v = 0.5 * v * (1.0 + jnp.tanh(0.7978845608 * (v + 0.044715 * (v * v * v))))
        v = v.astype(BF16).astype(F32)
        y_loc[m] = v
        total = total + jnp.sum(v * v, axis=1, keepdims=True)
    scale = lax.rsqrt(total * (1.0 / (n_tp * 128)) + 1e-6)
    for m in range(n_tp):
        owner = tp ^ m
        shaped[:, pl.ds(pl.multiple_of(owner * 128, 128), 128)] = (y_loc[m] * scale * ogain_ref[owner]).astype(BF16)
    loads[2].wait()
    for c in range(out_ref.shape[1] // COLS):
        at = slice(c * COLS, (c + 1) * COLS)
        out_ref[:, at] = jnp.dot(shaped[...], oproj[:, at], **FORM).astype(BF16)

    for copy in started:
        copy.wait_send()

    def drain(r, _):
        pltpu.make_async_copy(dt_send, dt_send, dt_ssem.at[r]).wait()
        for m in range(n_tp):
            pltpu.make_async_copy(e_send.at[m], e_send.at[m], e_ssem.at[r, m]).wait()
        return 0

    lax.fori_loop(rank + 1, n, drain, 0)


def on_device(
    tokens, step, in_gain, in_proj, decay_rate, frequency, input_map, readout, out_gain, out_proj
):
    n_tp, n_sp = lax.axis_size("tp"), lax.axis_size("sp")
    n = n_tp * n_sp
    rows, width = tokens.shape
    groups, size = decay_rate.shape
    lanes = groups * size
    inner = input_map.shape[3]
    chans = groups * inner
    assert n_tp == 4 and chans == 128 and inner == 16 and lax.axis_size("grp") == 2
    own_step = lax.dynamic_slice(step, (lax.axis_index("tp") * rows,), (rows,)).reshape(1, rows)
    rate, freq = decay_rate.reshape(1, lanes), frequency.reshape(1, lanes)
    rf = jnp.concatenate([rate, freq * (0.5 / math.pi)], axis=0)
    maps = input_map.transpose(0, 3, 1, 2).reshape(2, inner, lanes)
    norm = 1.0 / (rate * rate + freq * freq)
    b_re = (freq * maps[1] - rate * maps[0]) * norm
    b_im = -(freq * maps[0] + rate * maps[1]) * norm
    reads = readout.transpose(0, 2, 1, 3).reshape(2, inner, lanes)
    bc = jnp.stack([jnp.stack([b_re, b_im]), reads]).astype(BF16)
    vmem, dma = pltpu.VMEM, pltpu.SemaphoreType.DMA
    full = pl.BlockSpec(memory_space=pltpu.VMEM)
    away = pl.BlockSpec(memory_space=pl.ANY)
    tile = (2 * lanes // 128, 128)
    return pl.pallas_call(
        functools.partial(kernel, n, n_tp),
        out_shape=jax.ShapeDtypeStruct((rows, width), BF16),
        in_specs=[away, full, full, away, full, full, full, away],
        out_specs=full,
        scratch_shapes=[
            vmem((rows, width), BF16), vmem((rows, width), BF16), vmem((n_tp, width, chans), BF16),
            vmem((n_tp * chans, width), BF16),
            vmem((n_tp, rows, lanes), F32), vmem((n_tp, rows, lanes), F32),
            vmem((n_tp, rows, lanes), F32), vmem((n_tp, rows, lanes), F32),
            vmem((n_tp, rows, 2 * lanes), BF16),
            vmem((n_tp, rows, chans), F32),
            vmem((rows, 2 * lanes), BF16), vmem((rows, 2 * lanes), F32), vmem((rows, 2 * lanes), BF16),
            vmem((rows, 128), F32), vmem((n_tp, 2, lanes), F32), vmem((n_tp, 2, 2, inner, lanes), BF16),
            vmem((n_tp, 2) + tile, F32),
            vmem((n_tp,) + tile, F32), vmem((n, n_tp) + tile, F32),
            vmem((1, 128), F32), vmem((n, 1, 128), F32),
            vmem((n, n_tp) + tile, F32), vmem((n, n_tp) + tile, F32), vmem(tile, F32),
            vmem((chans, 2 * lanes), BF16), vmem((rows, n_tp * chans), BF16),
            dma((3,)), dma((n_tp,)), dma((n_tp,)), dma((5, CHUNKS)), dma((5, CHUNKS)), dma((5,)), dma((5,)),
            dma((n, n_tp)), dma((n, n_tp)), dma((n,)), dma((n,)),
        ],
        compiler_params=pltpu.CompilerParams(collective_id=0, has_side_effects=True, vmem_limit_bytes=60 * 2**20),
    )(tokens, own_step, in_gain.reshape(1, width), in_proj, rf, bc, out_gain.reshape(n_tp, 1, chans), out_proj)


def solution(mesh):
    placed = (
        P(("grp", "sp", "tp"), None),
        P(("grp", "sp")),
        P(),
        P(None, "tp"),
        P("tp", None),
        P("tp", None),
        P(None, "tp", None, None),
        P(None, "tp", None, None),
        P(),
        P(),
    )
    return jax.shard_map(
        on_device,
        mesh=mesh,
        in_specs=placed,
        out_specs=P(("grp", "sp", "tp"), None),
        check_vma=False,
    )
```

time: 309 us -> 49.9 us (0.16)
  the two profiles are of different devices: /device:TPU:0 before, /device:TPU:27 now
where the time goes in v1:
time: 49.9 us; the launch traced here: 49.4 us
  Pallas kernels  39.3 us (79%)
  local copies, waits for them, and re-layouts  7.22 us (14%)
  other arithmetic  2.87 us (6%)
    pallas_call x1, Pallas kernels, on_device(): pl.pallas_call(functools.partial(kernel, n, n_tp), out_shape=jax.ShapeDty...  39.3 us
    unnamed x1, local copies, waits for them, and re-layouts  2.3 us
    mul x2, local copies, waits for them, and re-layouts, on_device(): b_re = (freq * maps[1] - rate * maps[0]) * norm  1.52 us
    dynamic_slice x1, local copies, waits for them, and re-layouts, on_device(): lax.dynamic_slice(step, (lax.axis_index('tp') * rows,), (rows,))  1.33 us

profile of v1, /device:TPU:27, one launch (start us, length us, event | category | flops | bytes accessed | tf_op | source)
XLA Modules:
  0.0 49.4 jit_solution(9484638968044698724)
XLA Ops:
  0.0 1.3 %dynamic_slice.3 = f32[256]{0:T(256)} dynamic-slice(f32[1024]{0:T(1024)} %param.11, s32[]{:T(128)S(6)} %select_n.3), dynamic_slice_sizes={256} | dynamic-slice | bytes 2052 | tf_op jit(solution)/shard_map/dynamic_slice | solution.py:328
  1.3 0.8 %mul.131 = f32[512]{0:T(512)S(1)} reshape(f32[8,64]{1,0:T(8,128)} %param.14) | data formatting | bytes 4096 | tf_op jit(solution)/shard_map/mul | solution.py:333
  2.1 0.8 %mul.128 = f32[512]{0:T(512)S(1)} reshape(f32[8,64]{1,0:T(8,128)} %param.15) | data formatting | bytes 4096 | tf_op jit(solution)/shard_map/mul | solution.py:333
  2.9 0.8 %reshape.247 = f32[1,512]{1,0:T(1,128)S(1)} reshape(f32[8,64]{1,0:T(8,128)} %param.14) | data formatting | bytes 4096 | tf_op jit(solution)/shard_map/reshape | solution.py:329
  3.6 0.7 %broadcast_multiply_fusion = f32[8,64]{1,0:T(8,128)S(1)} fusion(f32[8,64]{1,0:T(8,128)} %param.15), kind=kLoop, calls=%fused_computation.7 | loop fusion | flops 512 | bytes 4096 | tf_op jit(solution)/shard_map/mul | solution.py:330
  4.3 0.1 mul.127
  4.4 0.6 %pad_maximum_fusion.1.rf_ref = f32[2,512]{1,0:T(2,128)} fusion(f32[1,512]{1,0:T(1,128)S(1)} %mul.127, f32[1,512]{1,0:T(1,128)S(1)} %reshape.247), kind=kLoop, calls=%fused_computation.5 | loop fusion | flops 1024 | bytes 8192 | tf_op jit(solution)/shard_map/concatenate | solution.py:330
  5.0 0.9 %convert_bitcast_fusion = bf16[2,16,8,64]{3,1,2,0:T(8,128)(2,1)S(1)} fusion(f32[2,8,16,64]{3,2,1,0:T(8,128)} %param.17), kind=kLoop, calls=%fused_computation.1 | loop fusion | flops 16384 | bytes 98304 | tf_op jit(solution)/shard_map/transpose | solution.py:335
  5.9 0.1 stack_reshape.4
  6.1 0.9 %fusion = (f32[1,16,8,64]{3,1,2,0:T(8,128)S(1)}, f32[1,16,8,64]{3,1,2,0:T(8,128)S(1)}) fusion(f32[2,16,8,64]{3,1,2,0:T(8,128)} %bitcast.14), kind=kLoop, calls=%fused_computation.8 | loop fusion | bytes 131072 | tf_op jit(solution)/shard_map/slice | solution.py:333
  7.0 0.1 squeeze.9
  7.1 0.1 squeeze.8
  7.2 0.6 %pad_maximum_fusion.bc_ref = bf16[2,2,16,512]{3,2,1,0:T(8,128)(2,1)} fusion(bf16[1,2,16,512]{3,2,1,0:T(8,128)(2,1)S(1)} %stack_reshape.4, bf16[1,2,16,512]{3,2,1,0:T(8,128)(2,1)S(1)} %maximum_bitcast_fusion), kind=kLoop, calls=%fused_computation | loop fusion | flops 32768 | bytes 131072 | tf_op jit(solution)/shard_map/stack | solution.py:336
  7.8 39.3 %shard_map.100 = bf16[256,2048]{1,0:T(8,128)(2,1)} custom-call(bf16[256,2048]{1,0:T(8,128)(2,1)} %tok_hbm.1, f32[1,256]{1,0:T(1,128)} %bitcast.16, f32[1,2048]{1,0:T(1,128)} %bitcast.15, bf16[2048,128]{1,0:T(8,128)(2,1)} %proj_hbm.1, f32[2,512]{1,0:T(2,128)} %pad_maximum_fusion.1.rf_ref, bf16[2,2,16,512]{3,2,1,0:T(8,128)(2,1)} %pad_maximum_fusion.bc_ref, ...), custom_call_target="tpu_custom_call" | custom-call | tf_op jit(solution)/shard_map/pallas_call | solution.py:341
  47.1 2.3 %copy.15 = bf16[256,2048]{1,0:T(8,128)(2,1)} copy(bf16[256,2048]{1,0:T(8,128)(2,1)} %shard_map.100) | data formatting | bytes 2097152
  (6 shorter events, 0.1 us)

commit v2 on v1

--- a/solution.py
+++ b/solution.py
@@ -13,9 +13,9 @@
 MESH = pl.DeviceIdType.MESH
 CHUNKS = 4
 STRIP = 16
-COLS = 512
 COS = (0.9999992107823232, -19.738980355764078, 64.9286574210355, -85.2716215343227, 58.79049212023138, -21.071105627794083)
 SIN = (6.28318491649543, -41.34158923268886, 81.59994332979169, -76.61447253134615, 41.34288235500672, -12.471243535733244)
+WHOLE = 12582912.0
 FORM = dict(preferred_element_type=F32)
 
 
@@ -27,16 +27,16 @@
 
 
 def turn(phase):
-    r = phase - jnp.round(phase)
+    r = phase - ((phase + WHOLE) - WHOLE)
     z = r * r
     return poly(COS, z), poly(SIN, z) * r
 
 
 def kernel(
-    n, n_tp, tok_hbm, step_ref, gain_ref, proj_hbm, rf_ref, bc_ref, ogain_ref, oproj_hbm, out_ref,
-    tok, normed, w_in, oproj, p_re, p_im, d_re, d_im, p_cat, y_loc,
-    wide, acc, state, times, rf_all, bc_all, rf8, e_send, e_recv, dt_send, dt_recv,
-    c_w, s_w, x_ref, tab, shaped,
+    n, n_tp, tok_hbm, step_ref, gain_ref, proj_hbm, rate_ref, freq_ref, map_ref, read_ref, ogain_ref, out_ref,
+    tok, normed, w_in, p_re, p_im, d_re, d_im, p_cat, y_loc,
+    wide, acc, state, times, rf_pack, rf_all, bc_all, rf8, e_send, e_recv, dt_send, dt_recv,
+    c_w, s_w, x_ref, tab,
     load_sem, small_sem, small_send, w_recv, w_send, bc_recv, bc_send,
     e_rsem, e_ssem, dt_rsem, dt_ssem,
 ):
@@ -58,7 +58,6 @@
     loads = [
         pltpu.make_async_copy(proj_hbm, w_in.at[0], load_sem.at[0]),
         pltpu.make_async_copy(tok_hbm, tok, load_sem.at[1]),
-        pltpu.make_async_copy(oproj_hbm, oproj, load_sem.at[2]),
     ]
     for copy in loads:
         copy.start()
@@ -72,7 +71,7 @@
     lax.fori_loop(1, n, greet, 0)
     pl.semaphore_signal(barrier, inc=1, device_id=across, device_id_type=MESH)
 
-    step_row = step_ref[...]
+    step_row = step_ref[:, pl.ds(pl.multiple_of(tp * rows, 128), rows)]
     row_id = lax.broadcasted_iota(jnp.int32, (rows, rows), 0)
     col_id = lax.broadcasted_iota(jnp.int32, (rows, rows), 1)
     causal = col_id <= row_id
@@ -81,6 +80,21 @@
     dt_send[...] = jnp.broadcast_to(jnp.sum(step_row, axis=1, keepdims=True), (1, 128))
     lower = causal.astype(F32).astype(BF16)
 
+    size = rate_ref.shape[1]
+    per = map_ref.shape[1] // rate_ref.shape[0]
+    rate, freq = rate_ref[...], freq_ref[...]
+    rf_pack[0] = jnp.concatenate([rate, freq * (0.5 / math.pi)], axis=1)
+
+    def rows_of(value):
+        return jnp.concatenate([jnp.broadcast_to(value[g:g + 1], (per, size)) for g in range(value.shape[0])], axis=0)
+
+    norm = 1.0 / (rate * rate + freq * freq)
+    r_n, f_n = rows_of(-rate * norm), rows_of(freq * norm)
+    bc_all[0, 0] = jnp.concatenate(
+        [f_n * map_ref[1] + r_n * map_ref[0], r_n * map_ref[1] - f_n * map_ref[0]], axis=1
+    ).astype(BF16)
+    bc_all[0, 1] = jnp.concatenate([read_ref[0], read_ref[1]], axis=1).astype(BF16)
+
     loads[0].wait()
     pl.semaphore_wait(barrier, n)
 
@@ -98,15 +112,15 @@
         pltpu.make_async_copy(dst, dst, rsem).wait()
 
     for m in range(1, n_tp):
-        send(rf_ref, rf_all.at[m], small_send.at[m], small_sem.at[m], peer[m])
+        send(rf_pack.at[0], rf_pack.at[m], small_send.at[m], small_sem.at[m], peer[m])
     own_half = grp * half
     other_half = (1 - grp) * half
     for c in range(CHUNKS):
         part = pl.ds(pl.multiple_of(own_half + c * piece, 128), piece)
         send(w_in.at[0, part], w_in.at[2, part], w_send.at[0, c], w_recv.at[0, c], peer[2])
     send(w_in.at[0], w_in.at[1], w_send.at[1, 0], w_recv.at[1, 0], peer[1])
-    send(bc_ref.at[grp], bc_all.at[2, grp], bc_send.at[0], bc_recv.at[0], peer[2])
-    send(bc_ref, bc_all.at[1], bc_send.at[1], bc_recv.at[1], peer[1])
+    send(bc_all.at[0, grp], bc_all.at[2, grp], bc_send.at[0], bc_recv.at[0], peer[2])
+    send(bc_all.at[0], bc_all.at[1], bc_send.at[1], bc_recv.at[1], peer[1])
 
     def send_times(r, _):
         copy = pltpu.make_async_remote_copy(
@@ -118,8 +132,20 @@
 
     lax.fori_loop(rank + 1, n, send_times, 0)
 
-    rf_all[0] = rf_ref[...]
-    bc_all[0] = bc_ref[...]
+    left = lax.broadcasted_iota(jnp.int32, (1, 128), 1) < size
+
+    def unpack_rates(m):
+        pack = rf_pack[m]
+        flip = pltpu.roll(pack, size, 1)
+        for kind in range(2):
+            near, far = (pack, flip) if kind == 0 else (flip, pack)
+            for b in range(blocks):
+                row = jnp.where(left, near[2 * b:2 * b + 1], far[2 * b + 1:2 * b + 2])
+                rf_all[m, kind:kind + 1, b * 128:(b + 1) * 128] = row
+                rf8[m, kind, pl.ds(b, 1), :] = row
+                rf8[m, kind, pl.ds(blocks + b, 1), :] = row
+
+    unpack_rates(0)
 
     loads[1].wait()
     gain = gain_ref[...]
@@ -167,17 +193,19 @@
 
         lax.fori_loop(0, rows // STRIP, strip, (jnp.ones((STRIP, lanes), F32), jnp.zeros((STRIP, lanes), F32)))
 
-    per = 16
-    mask_r = lax.broadcasted_iota(jnp.int32, (128, lanes), 0) // per
-    mask_c = lax.broadcasted_iota(jnp.int32, (128, lanes), 1) // (lanes // (128 // per))
-    same = mask_r == mask_c
-
-    def spread(compact):
-        return jnp.where(same, jnp.concatenate([compact.astype(F32)] * (128 // per), axis=0), 0.0)
+    mask_r = lax.broadcasted_iota(jnp.int32, (128, 128), 0) // per
+    mask_c = lax.broadcasted_iota(jnp.int32, (128, 128), 1) // size
+    same = [mask_r == mask_c + 2 * b for b in range(blocks)]
+
+    def spread(packed):
+        value = packed.astype(F32)
+        flip = pltpu.roll(value, size, 1)
+        re, im = jnp.where(left, value, flip), jnp.where(left, flip, value)
+        return [jnp.where(keep, re, 0.0) for keep in same], [jnp.where(keep, im, 0.0) for keep in same]
 
     def local(m):
-        tab[:, 0:lanes] = spread(bc_all[m, 0, 0]).astype(BF16)
-        tab[:, lanes:] = spread(bc_all[m, 0, 1]).astype(BF16)
+        re, im = spread(bc_all[m, 0])
+        tab[...] = jnp.concatenate(re + im, axis=1).astype(BF16)
         drive = jnp.dot(normed[...], w_in[m], **FORM).astype(BF16)
         acc[...] = jnp.dot(drive, tab[...], **FORM)
 
@@ -219,14 +247,15 @@
             return 0
 
         lax.fori_loop(0, rows // STRIP, rotate, 0)
-        tab[:, 0:lanes] = spread(bc_all[m, 1, 0]).astype(BF16)
-        tab[:, lanes:] = (-spread(bc_all[m, 1, 1])).astype(BF16)
+        re, im = spread(bc_all[m, 1])
+        tab[...] = jnp.concatenate(re + [-value for value in im], axis=1).astype(BF16)
         y_loc[m] = lax.dot_general(state[...], tab[...], (((1,), (1,)), ((), ())), **FORM)
 
     tables(0)
     local(0)
     for m in range(1, n_tp):
-        arrived(rf_all.at[m], small_sem.at[m])
+        arrived(rf_pack.at[m], small_sem.at[m])
+        unpack_rates(m)
     tables(1)
     for c in range(CHUNKS):
         forward(c, True)
@@ -244,14 +273,6 @@
     tables(3)
     local(2)
     sign = jnp.where(lax.broadcasted_iota(jnp.int32, (2 * blocks, 128), 0) < blocks, -1.0, 1.0)
-    for m in range(n_tp):
-        for b in range(blocks):
-            at = pl.ds(b * 128, 128)
-            for kind in range(2):
-                value = rf_all[m, kind:kind + 1, at]
-                rf8[m, kind, pl.ds(b, 1), :] = value
-                rf8[m, kind, pl.ds(blocks + b, 1), :] = value
-
     def weight(k, since):
         j = rank - 1 - k
         arrived(dt_recv.at[j], dt_rsem.at[j])
@@ -281,13 +302,11 @@
             return x + c_w[j, m] * value + s_w[j, m] * pltpu.roll(value, blocks, 0)
 
         x_ref[...] = lax.fori_loop(0, rank, take, jnp.zeros((2 * blocks, 128), F32))
-        cr = spread(bc_all[m, 1, 0])
-        ci = spread(bc_all[m, 1, 1])
+        cr, ci = spread(bc_all[m, 1])
         for b in range(blocks):
-            at = slice(b * 128, (b + 1) * 128)
             xr, xi = x_ref[pl.ds(b, 1), :], x_ref[pl.ds(blocks + b, 1), :]
-            tab[:, b * 128:(b + 1) * 128] = (cr[:, at] * xr - ci[:, at] * xi).astype(BF16)
-            tab[:, lanes + b * 128:lanes + (b + 1) * 128] = (-(cr[:, at] * xi + ci[:, at] * xr)).astype(BF16)
+            tab[:, b * 128:(b + 1) * 128] = (cr[b] * xr - ci[b] * xi).astype(BF16)
+            tab[:, lanes + b * 128:lanes + (b + 1) * 128] = (-(cr[b] * xi + ci[b] * xr)).astype(BF16)
         v = y_loc[m] + lax.dot_general(p_cat[m], tab[...], (((1,), (1,)), ((), ())), **FORM)
         v = 0.5 * v * (1.0 + jnp.tanh(0.7978845608 * (v + 0.044715 * (v * v * v))))
         v = v.astype(BF16).astype(F32)
@@ -296,12 +315,7 @@
     scale = lax.rsqrt(total * (1.0 / (n_tp * 128)) + 1e-6)
     for m in range(n_tp):
         owner = tp ^ m
-        shaped[:, pl.ds(pl.multiple_of(owner * 128, 128), 128)] = (y_loc[m] * scale * ogain_ref[owner]).astype(BF16)
-    loads[2].wait()
-    for c in range(out_ref.shape[1] // COLS):
-        at = slice(c * COLS, (c + 1) * COLS)
-        out_ref[:, at] = jnp.dot(shaped[...], oproj[:, at], **FORM).astype(BF16)
-
+        out_ref[:, pl.ds(pl.multiple_of(owner * 128, 128), 128)] = (y_loc[m] * scale * ogain_ref[owner]).astype(BF16)
     for copy in started:
         copy.wait_send()
 
@@ -324,44 +338,41 @@
     lanes = groups * size
     inner = input_map.shape[3]
     chans = groups * inner
-    assert n_tp == 4 and chans == 128 and inner == 16 and lax.axis_size("grp") == 2
-    own_step = lax.dynamic_slice(step, (lax.axis_index("tp") * rows,), (rows,)).reshape(1, rows)
-    rate, freq = decay_rate.reshape(1, lanes), frequency.reshape(1, lanes)
-    rf = jnp.concatenate([rate, freq * (0.5 / math.pi)], axis=0)
-    maps = input_map.transpose(0, 3, 1, 2).reshape(2, inner, lanes)
-    norm = 1.0 / (rate * rate + freq * freq)
-    b_re = (freq * maps[1] - rate * maps[0]) * norm
-    b_im = -(freq * maps[0] + rate * maps[1]) * norm
-    reads = readout.transpose(0, 2, 1, 3).reshape(2, inner, lanes)
-    bc = jnp.stack([jnp.stack([b_re, b_im]), reads]).astype(BF16)
+    assert n_tp == 4 and chans == 128 and size == 64 and groups == 8 and lax.axis_size("grp") == 2
+    maps = input_map.transpose(0, 1, 3, 2).reshape(2, chans, size)
+    reads = readout.reshape(2, chans, size)
     vmem, dma = pltpu.VMEM, pltpu.SemaphoreType.DMA
     full = pl.BlockSpec(memory_space=pltpu.VMEM)
     away = pl.BlockSpec(memory_space=pl.ANY)
     tile = (2 * lanes // 128, 128)
-    return pl.pallas_call(
+    shaped = pl.pallas_call(
         functools.partial(kernel, n, n_tp),
-        out_shape=jax.ShapeDtypeStruct((rows, width), BF16),
-        in_specs=[away, full, full, away, full, full, full, away],
+        out_shape=jax.ShapeDtypeStruct((rows, n_tp * chans), BF16),
+        in_specs=[away, full, full, away, full, full, full, full, full],
         out_specs=full,
         scratch_shapes=[
             vmem((rows, width), BF16), vmem((rows, width), BF16), vmem((n_tp, width, chans), BF16),
-            vmem((n_tp * chans, width), BF16),
             vmem((n_tp, rows, lanes), F32), vmem((n_tp, rows, lanes), F32),
             vmem((n_tp, rows, lanes), F32), vmem((n_tp, rows, lanes), F32),
             vmem((n_tp, rows, 2 * lanes), BF16),
             vmem((n_tp, rows, chans), F32),
             vmem((rows, 2 * lanes), BF16), vmem((rows, 2 * lanes), F32), vmem((rows, 2 * lanes), BF16),
-            vmem((rows, 128), F32), vmem((n_tp, 2, lanes), F32), vmem((n_tp, 2, 2, inner, lanes), BF16),
+            vmem((rows, 128), F32), vmem((n_tp, groups, 2 * size), F32), vmem((n_tp, 2, lanes), F32),
+            vmem((n_tp, 2, chans, 2 * size), BF16),
             vmem((n_tp, 2) + tile, F32),
             vmem((n_tp,) + tile, F32), vmem((n, n_tp) + tile, F32),
             vmem((1, 128), F32), vmem((n, 1, 128), F32),
             vmem((n, n_tp) + tile, F32), vmem((n, n_tp) + tile, F32), vmem(tile, F32),
-            vmem((chans, 2 * lanes), BF16), vmem((rows, n_tp * chans), BF16),
-            dma((3,)), dma((n_tp,)), dma((n_tp,)), dma((5, CHUNKS)), dma((5, CHUNKS)), dma((5,)), dma((5,)),
+            vmem((chans, 2 * lanes), BF16),
+            dma((2,)), dma((n_tp,)), dma((n_tp,)), dma((5, CHUNKS)), dma((5, CHUNKS)), dma((5,)), dma((5,)),
             dma((n, n_tp)), dma((n, n_tp)), dma((n,)), dma((n,)),
         ],
         compiler_params=pltpu.CompilerParams(collective_id=0, has_side_effects=True, vmem_limit_bytes=60 * 2**20),
-    )(tokens, own_step, in_gain.reshape(1, width), in_proj, rf, bc, out_gain.reshape(n_tp, 1, chans), out_proj)
+    )(
+        tokens, step.reshape(1, -1), in_gain.reshape(1, width), in_proj, decay_rate, frequency, maps, reads,
+        out_gain.reshape(n_tp, 1, chans),
+    )
+    return jnp.dot(shaped, out_proj, preferred_element_type=F32).astype(BF16)
 
 
 def solution(mesh):

time: 49.9 us -> 42.4 us (0.85)
  local copies, waits for them, and re-layouts: 7.22 us -> 0.01 us
  other arithmetic: 2.87 us -> 0 us
  matrix products: 0 us -> 2.64 us
    dot_general x0 -> x1, matrix products: none -> 2.64 us  [on_device(): return jnp.dot(shaped, out_proj, preferred_element_type=F32).astype(BF16)]
    unnamed x1 -> x2, local copies, waits for them, and re-layouts: 2.3 us -> 0.01 us
    mul x3 -> x0, local copies, waits for them, and re-layouts: 1.6 us -> none  [the longest x2 1.52 us: on_device(): b_re = (freq * maps[1] - rate * maps[0]) * norm]
    dynamic_slice x1 -> x0, local copies, waits for them, and re-layouts: 1.33 us -> none  [on_device(): lax.dynamic_slice(step, (lax.axis_index('tp') * rows,), (rows,))]
    slice x3 -> x0, local copies, waits for them, and re-layouts: 0.93 us -> none  [on_device(): b_re = (freq * maps[1] - rate * maps[0]) * norm]
    transpose x1 -> x0, other arithmetic: 0.91 us -> none  [on_device(): reads = readout.transpose(0, 2, 1, 3).reshape(2, inner, lanes)]
    reshape x1 -> x0, local copies, waits for them, and re-layouts: 0.77 us -> none  [on_device(): rate, freq = (decay_rate.reshape(1, lanes), frequency.reshape(1, lanes))]
    mul x1 -> x0, other arithmetic: 0.69 us -> none  [on_device(): rf = jnp.concatenate([rate, freq * (0.5 / math.pi)], axis=0)]
where the time goes in v2:
time: 42.4 us; the launch traced here: 42.2 us
  Pallas kernels  39.5 us (93%)
  matrix products  2.64 us (6%)
    pallas_call x1, Pallas kernels, on_device(): pl.pallas_call(functools.partial(kernel, n, n_tp), out_shape=jax.ShapeDty...  39.5 us
    dot_general x1, matrix products, on_device(): return jnp.dot(shaped, out_proj, preferred_element_type=F32).astype(BF16)  2.64 us

profile of v2, /device:TPU:27, one launch (start us, length us, event | category | flops | bytes accessed | tf_op | source)
XLA Modules:
  0.0 42.2 jit_solution(13061554853234333815)
XLA Ops:
  0.0 0.0 copy-start
  0.0 39.5 %shard_map.100 = bf16[256,512]{1,0:T(8,128)(2,1)} custom-call(bf16[256,2048]{1,0:T(8,128)(2,1)} %tok_hbm.1, f32[1,1024]{1,0:T(1,128)} %bitcast.12, f32[1,2048]{1,0:T(1,128)} %bitcast.11, bf16[2048,128]{1,0:T(8,128)(2,1)} %proj_hbm.1, f32[8,64]{1,0:T(8,128)} %rate_ref.1, f32[8,64]{1,0:T(8,128)} %freq_ref.1, f32[2,128,64]{2,1,0:T(8,128)} %bitcast.9, ...), custom_call_target="tpu_custom_call" | custom-call | tf_op jit(solution)/shard_map/pallas_call | solution.py:348
  39.5 0.0 copy-done
  39.6 2.6 %convolution_convert_fusion = bf16[256,2048]{1,0:T(8,128)(2,1)} fusion(bf16[256,512]{1,0:T(8,128)(2,1)} %shard_map.100, bf16[512,2048]{1,0:T(8,128)(2,1)S(1)} %copy-done), kind=kOutput, calls=%fused_computation | convolution fusion | flops 537395200 | bytes 3407872 | tf_op jit(solution)/shard_map/dot_general | solution.py:375
Async XLA Ops:
  0.0 39.5 %copy-start = (bf16[512,2048]{1,0:T(8,128)(2,1)S(1)}, bf16[512,2048]{1,0:T(8,128)(2,1)}, u32[]{:S(2)}) copy-start(bf16[512,2048]{1,0:T(8,128)(2,1)} %param.19) | copy-start | bytes 6291460

commit v3 on v2

--- a/solution.py
+++ b/solution.py
@@ -13,6 +13,7 @@
 MESH = pl.DeviceIdType.MESH
 CHUNKS = 4
 STRIP = 16
+UNROLL = 4
 COS = (0.9999992107823232, -19.738980355764078, 64.9286574210355, -85.2716215343227, 58.79049212023138, -21.071105627794083)
 SIN = (6.28318491649543, -41.34158923268886, 81.59994332979169, -76.61447253134615, 41.34288235500672, -12.471243535733244)
 WHOLE = 12582912.0
@@ -36,7 +37,7 @@
     n, n_tp, tok_hbm, step_ref, gain_ref, proj_hbm, rate_ref, freq_ref, map_ref, read_ref, ogain_ref, out_ref,
     tok, normed, w_in, p_re, p_im, d_re, d_im, p_cat, y_loc,
     wide, acc, state, times, rf_pack, rf_all, bc_all, rf8, e_send, e_recv, dt_send, dt_recv,
-    c_w, s_w, x_ref, tab,
+    c_w, s_w, x_ref, tab, drive, c_tab,
     load_sem, small_sem, small_send, w_recv, w_send, bc_recv, bc_send,
     e_rsem, e_ssem, dt_rsem, dt_ssem,
 ):
@@ -95,43 +96,6 @@
     ).astype(BF16)
     bc_all[0, 1] = jnp.concatenate([read_ref[0], read_ref[1]], axis=1).astype(BF16)
 
-    loads[0].wait()
-    pl.semaphore_wait(barrier, n)
-
-    started = []
-
-    def send(src, dst, ssem, rsem, where):
-        copy = pltpu.make_async_remote_copy(
-            src_ref=src, dst_ref=dst, send_sem=ssem, recv_sem=rsem, device_id=where, device_id_type=MESH
-        )
-        copy.start()
-        started.append(copy)
-        return copy
-
-    def arrived(dst, rsem):
-        pltpu.make_async_copy(dst, dst, rsem).wait()
-
-    for m in range(1, n_tp):
-        send(rf_pack.at[0], rf_pack.at[m], small_send.at[m], small_sem.at[m], peer[m])
-    own_half = grp * half
-    other_half = (1 - grp) * half
-    for c in range(CHUNKS):
-        part = pl.ds(pl.multiple_of(own_half + c * piece, 128), piece)
-        send(w_in.at[0, part], w_in.at[2, part], w_send.at[0, c], w_recv.at[0, c], peer[2])
-    send(w_in.at[0], w_in.at[1], w_send.at[1, 0], w_recv.at[1, 0], peer[1])
-    send(bc_all.at[0, grp], bc_all.at[2, grp], bc_send.at[0], bc_recv.at[0], peer[2])
-    send(bc_all.at[0], bc_all.at[1], bc_send.at[1], bc_recv.at[1], peer[1])
-
-    def send_times(r, _):
-        copy = pltpu.make_async_remote_copy(
-            src_ref=dt_send, dst_ref=dt_recv.at[rank], send_sem=dt_ssem.at[r], recv_sem=dt_rsem.at[rank],
-            device_id=place(r), device_id_type=MESH,
-        )
-        copy.start()
-        return 0
-
-    lax.fori_loop(rank + 1, n, send_times, 0)
-
     left = lax.broadcasted_iota(jnp.int32, (1, 128), 1) < size
 
     def unpack_rates(m):
@@ -157,16 +121,7 @@
         normed[at, :] = (value * scale * gain).astype(BF16)
         return 0
 
-    lax.fori_loop(0, rows // STRIP, norm_strip, 0)
-
-    def forward(c, mine):
-        base = own_half if mine else other_half
-        part = pl.ds(pl.multiple_of(base + c * piece, 128), piece)
-        way = 0 if mine else 2
-        arrived(w_in.at[2, part], w_recv.at[way, c])
-        if mine:
-            send(w_in.at[2, part], w_in.at[2, part], w_send.at[2, c], w_recv.at[2, c], across)
-        send(w_in.at[2, part], w_in.at[3, part], w_send.at[3 if mine else 4, c], w_recv.at[3 if mine else 4, c], peer[1])
+    lax.fori_loop(0, rows // STRIP, norm_strip, 0, unroll=2)
 
     def tables(m):
         rate = rf_all[m, 0:1, :]
@@ -191,7 +146,54 @@
             d_im[m, at, :] = jnp.where(first, pltpu.roll(bi, 1, 0), pltpu.roll(qi, 1, 0)) - qi
             return qr, qi
 
-        lax.fori_loop(0, rows // STRIP, strip, (jnp.ones((STRIP, lanes), F32), jnp.zeros((STRIP, lanes), F32)))
+        lax.fori_loop(0, rows // STRIP, strip, (jnp.ones((STRIP, lanes), F32), jnp.zeros((STRIP, lanes), F32)), unroll=UNROLL)
+
+    tables(0)
+    loads[0].wait()
+    pl.semaphore_wait(barrier, n)
+
+    started = []
+
+    def send(src, dst, ssem, rsem, where):
+        copy = pltpu.make_async_remote_copy(
+            src_ref=src, dst_ref=dst, send_sem=ssem, recv_sem=rsem, device_id=where, device_id_type=MESH
+        )
+        copy.start()
+        started.append(copy)
+        return copy
+
+    def arrived(dst, rsem):
+        pltpu.make_async_copy(dst, dst, rsem).wait()
+
+    for m in range(1, n_tp):
+        send(rf_pack.at[0], rf_pack.at[m], small_send.at[m], small_sem.at[m], peer[m])
+    own_half = grp * half
+    other_half = (1 - grp) * half
+    for c in range(CHUNKS):
+        part = pl.ds(pl.multiple_of(own_half + c * piece, 128), piece)
+        send(w_in.at[0, part], w_in.at[2, part], w_send.at[0, c], w_recv.at[0, c], peer[2])
+    send(w_in.at[0], w_in.at[1], w_send.at[1, 0], w_recv.at[1, 0], peer[1])
+    send(bc_all.at[0, grp], bc_all.at[2, grp], bc_send.at[0], bc_recv.at[0], peer[2])
+    send(bc_all.at[0], bc_all.at[1], bc_send.at[1], bc_recv.at[1], peer[1])
+
+    def send_times(r, _):
+        copy = pltpu.make_async_remote_copy(
+            src_ref=dt_send, dst_ref=dt_recv.at[rank], send_sem=dt_ssem.at[r], recv_sem=dt_rsem.at[rank],
+            device_id=place(r), device_id_type=MESH,
+        )
+        copy.start()
+        return 0
+
+    lax.fori_loop(rank + 1, n, send_times, 0)
+
+    def forward(c, mine):
+        base = own_half if mine else other_half
+        part = pl.ds(pl.multiple_of(base + c * piece, 128), piece)
+        way = 0 if mine else 2
+        arrived(w_in.at[2, part], w_recv.at[way, c])
+        if mine:
+            send(w_in.at[2, part], w_in.at[2, part], w_send.at[2, c], w_recv.at[2, c], across)
+        send(w_in.at[2, part], w_in.at[3, part], w_send.at[3 if mine else 4, c], w_recv.at[3 if mine else 4, c], peer[1])
 
     mask_r = lax.broadcasted_iota(jnp.int32, (128, 128), 0) // per
     mask_c = lax.broadcasted_iota(jnp.int32, (128, 128), 1) // size
@@ -203,11 +205,16 @@
         re, im = jnp.where(left, value, flip), jnp.where(left, flip, value)
         return [jnp.where(keep, re, 0.0) for keep in same], [jnp.where(keep, im, 0.0) for keep in same]
 
+    def project(m):
+        pair = jnp.concatenate([w_in[m], w_in[m + 1]], axis=1)
+        value = jnp.dot(normed[...], pair, **FORM).astype(BF16)
+        drive[m] = value[:, 0:128]
+        drive[m + 1] = value[:, 128:]
+
     def local(m):
         re, im = spread(bc_all[m, 0])
         tab[...] = jnp.concatenate(re + im, axis=1).astype(BF16)
-        drive = jnp.dot(normed[...], w_in[m], **FORM).astype(BF16)
-        acc[...] = jnp.dot(drive, tab[...], **FORM)
+        acc[...] = jnp.dot(drive[m], tab[...], **FORM)
 
         def weigh(i, _):
             at = pl.ds(pl.multiple_of(i * STRIP, STRIP), STRIP)
@@ -217,7 +224,7 @@
             wide[at, lanes:] = (dr * vi + di * vr).astype(BF16)
             return 0
 
-        lax.fori_loop(0, rows // STRIP, weigh, 0)
+        lax.fori_loop(0, rows // STRIP, weigh, 0, unroll=4)
         acc[...] = jnp.dot(lower, wide[...], **FORM)
         last = pl.ds(rows - 1, 1)
         for b in range(blocks):
@@ -246,32 +253,38 @@
             state[at, lanes:] = (pr * ai + pi * ar).astype(BF16)
             return 0
 
-        lax.fori_loop(0, rows // STRIP, rotate, 0)
+        lax.fori_loop(0, rows // STRIP, rotate, 0, unroll=4)
         re, im = spread(bc_all[m, 1])
+        for b in range(blocks):
+            c_tab[m, :, b * 128:(b + 1) * 128] = re[b]
+            c_tab[m, :, lanes + b * 128:lanes + (b + 1) * 128] = im[b]
         tab[...] = jnp.concatenate(re + [-value for value in im], axis=1).astype(BF16)
         y_loc[m] = lax.dot_general(state[...], tab[...], (((1,), (1,)), ((), ())), **FORM)
 
-    tables(0)
-    local(0)
     for m in range(1, n_tp):
         arrived(rf_pack.at[m], small_sem.at[m])
         unpack_rates(m)
     tables(1)
-    for c in range(CHUNKS):
-        forward(c, True)
+    forward(0, True)
+    tables(2)
+    forward(1, True)
+    arrived(w_in.at[1], w_recv.at[1, 0])
+    arrived(bc_all.at[1], bc_recv.at[1])
+    project(0)
+    local(0)
+    forward(2, True)
+    forward(3, True)
     arrived(bc_all.at[2, grp], bc_recv.at[0])
     send(bc_all.at[2, grp], bc_all.at[2, grp], bc_send.at[2], bc_recv.at[2], across)
     send(bc_all.at[2, grp], bc_all.at[3, grp], bc_send.at[3], bc_recv.at[3], peer[1])
-    tables(2)
-    for c in range(CHUNKS):
-        forward(c, False)
+    local(1)
+    forward(0, False)
+    forward(1, False)
+    forward(2, False)
+    tables(3)
+    forward(3, False)
     arrived(bc_all.at[2, 1 - grp], bc_recv.at[2])
     send(bc_all.at[2, 1 - grp], bc_all.at[3, 1 - grp], bc_send.at[4], bc_recv.at[4], peer[1])
-    arrived(w_in.at[1], w_recv.at[1, 0])
-    arrived(bc_all.at[1], bc_recv.at[1])
-    local(1)
-    tables(3)
-    local(2)
     sign = jnp.where(lax.broadcasted_iota(jnp.int32, (2 * blocks, 128), 0) < blocks, -1.0, 1.0)
     def weight(k, since):
         j = rank - 1 - k
@@ -290,6 +303,8 @@
         arrived(w_in.at[3, pl.ds(pl.multiple_of(other_half + c * piece, 128), piece)], w_recv.at[4, c])
     arrived(bc_all.at[3, grp], bc_recv.at[3])
     arrived(bc_all.at[3, 1 - grp], bc_recv.at[4])
+    project(2)
+    local(2)
     local(3)
 
     total = jnp.zeros((rows, 1), F32)
@@ -302,11 +317,11 @@
             return x + c_w[j, m] * value + s_w[j, m] * pltpu.roll(value, blocks, 0)
 
         x_ref[...] = lax.fori_loop(0, rank, take, jnp.zeros((2 * blocks, 128), F32))
-        cr, ci = spread(bc_all[m, 1])
         for b in range(blocks):
+            cr, ci = c_tab[m, :, b * 128:(b + 1) * 128], c_tab[m, :, lanes + b * 128:lanes + (b + 1) * 128]
             xr, xi = x_ref[pl.ds(b, 1), :], x_ref[pl.ds(blocks + b, 1), :]
-            tab[:, b * 128:(b + 1) * 128] = (cr[b] * xr - ci[b] * xi).astype(BF16)
-            tab[:, lanes + b * 128:lanes + (b + 1) * 128] = (-(cr[b] * xi + ci[b] * xr)).astype(BF16)
+            tab[:, b * 128:(b + 1) * 128] = (cr * xr - ci * xi).astype(BF16)
+            tab[:, lanes + b * 128:lanes + (b + 1) * 128] = (-(cr * xi + ci * xr)).astype(BF16)
         v = y_loc[m] + lax.dot_general(p_cat[m], tab[...], (((1,), (1,)), ((), ())), **FORM)
         v = 0.5 * v * (1.0 + jnp.tanh(0.7978845608 * (v + 0.044715 * (v * v * v))))
         v = v.astype(BF16).astype(F32)
@@ -363,7 +378,7 @@
             vmem((n_tp,) + tile, F32), vmem((n, n_tp) + tile, F32),
             vmem((1, 128), F32), vmem((n, 1, 128), F32),
             vmem((n, n_tp) + tile, F32), vmem((n, n_tp) + tile, F32), vmem(tile, F32),
-            vmem((chans, 2 * lanes), BF16),
+            vmem((chans, 2 * lanes), BF16), vmem((n_tp, rows, chans), BF16), vmem((n_tp, chans, 2 * lanes), F32),
             dma((2,)), dma((n_tp,)), dma((n_tp,)), dma((5, CHUNKS)), dma((5, CHUNKS)), dma((5,)), dma((5,)),
             dma((n, n_tp)), dma((n, n_tp)), dma((n,)), dma((n,)),
         ],

time: 42.4 us -> 33.2 us (0.78)
  Pallas kernels: 39.5 us -> 30 us
    pallas_call x1, Pallas kernels: 39.5 us -> 30 us  [on_device(): pl.pallas_call(functools.partial(kernel, n, n_tp), out_shape=jax.ShapeDty...]
where the time goes in v3:
time: 33.2 us; the launch traced here: 32.7 us
  Pallas kernels  30 us (90%)
  matrix products  2.63 us (8%)
    pallas_call x1, Pallas kernels, on_device(): pl.pallas_call(functools.partial(kernel, n, n_tp), out_shape=jax.ShapeDty...  30 us
    dot_general x1, matrix products, on_device(): return jnp.dot(shaped, out_proj, preferred_element_type=F32).astype(BF16)  2.63 us

profile of v3, /device:TPU:27, one launch (start us, length us, event | category | flops | bytes accessed | tf_op | source)
XLA Modules:
  0.0 32.7 jit_solution(14739840202022504484)
XLA Ops:
  0.0 0.0 copy-start
  0.0 30.0 %shard_map.100 = bf16[256,512]{1,0:T(8,128)(2,1)} custom-call(bf16[256,2048]{1,0:T(8,128)(2,1)} %tok_hbm.1, f32[1,1024]{1,0:T(1,128)} %bitcast.12, f32[1,2048]{1,0:T(1,128)} %bitcast.11, bf16[2048,128]{1,0:T(8,128)(2,1)} %proj_hbm.1, f32[8,64]{1,0:T(8,128)} %rate_ref.1, f32[8,64]{1,0:T(8,128)} %freq_ref.1, f32[2,128,64]{2,1,0:T(8,128)} %bitcast.9, ...), custom_call_target="tpu_custom_call" | custom-call | tf_op jit(solution)/shard_map/pallas_call | solution.py:363
  30.0 0.0 copy-done
  30.0 2.6 %convolution_convert_fusion = bf16[256,2048]{1,0:T(8,128)(2,1)} fusion(bf16[256,512]{1,0:T(8,128)(2,1)} %shard_map.100, bf16[512,2048]{1,0:T(8,128)(2,1)S(1)} %copy-done), kind=kOutput, calls=%fused_computation | convolution fusion | flops 537395200 | bytes 3407872 | tf_op jit(solution)/shard_map/dot_general | solution.py:390
Async XLA Ops:
  0.0 30.0 %copy-start = (bf16[512,2048]{1,0:T(8,128)(2,1)S(1)}, bf16[512,2048]{1,0:T(8,128)(2,1)}, u32[]{:S(2)}) copy-start(bf16[512,2048]{1,0:T(8,128)(2,1)} %param.19) | copy-start | bytes 6291460
